TPU v7x, 768 devices: a whole 4x8x12 slice. The times are simulated.
768 devices in a mesh: sp: 16 (over y, core), dp: 48 (over z, x).
Axes of the slice: x: 4, y: 8, z: 12, core: 2. Of those that a mesh axis runs over, the one named last changes fastest.
Arguments:
- q_latent: bfloat16 [48, 2048, 512], P('dp', 'sp'), may hold values from -70 to 70
- kv_latent: bfloat16 [48, 2048, 512], P('dp', 'sp'), may hold values from -70 to 70
- rope_key: bfloat16 [48, 2048, 64], P('dp', 'sp'), may hold values from -370 to 370
- w_query: bfloat16 [512, 3072], P(None, 'dp'), may hold values from -0.25 to 0.25
- w_keyval: bfloat16 [512, 4096], P(None, 'sp'), may hold values from -0.25 to 0.25
- w_out: bfloat16 [2048, 2048], replicated, may hold values from -0.125 to 0.125
- query_gain: bfloat16 [512], replicated, may hold values from 0.099609375 to 1.8984375
- latent_gain: bfloat16 [512], replicated, may hold values from 0.099609375 to 1.8984375
- out_gain: bfloat16 [2048], replicated, may hold values from 0.099609375 to 1.8984375
Outputs:
- output: bfloat16 [48, 2048, 2048], P('dp', 'sp')
All inputs are finite; a program needn't handle non-finite values.
Results may differ from a plain program's by a relative error of at most 0.03.
The roundings to bfloat16 on the way count: a program that leaves them out, or rounds other values in their place, can miss the bound.
Values may be sent and summed in bfloat16 or wider, within the bound.
A program may use at most 64 MiB of HBM per device.

v0:
```python
import jax
import jax.numpy as jnp
from jax import lax
from jax.sharding import Mesh
from jax.sharding import PartitionSpec as P

H = 16
NOPE = 128
ROPE = 64
VDIM = 128
DP = ("dp_0", "dp_1")


def gather_axes(x, axes, dim):
    if not axes:
        return x
    nearer = lax.all_gather(x, axes[-1], axis=dim, tiled=True)
    return gather_axes(nearer, axes[:-1], dim)


def joined_along(blocks, dim):
    blocks = jnp.moveaxis(blocks, 0, dim)
    dims = blocks.shape
    return blocks.reshape(*dims[:dim], dims[dim] * dims[dim + 1], *dims[dim + 2 :])


def from_everyone(x, axis):
    peers = lax.axis_size(axis)
    return lax.all_to_all(jnp.broadcast_to(x[None], (peers, *x.shape)), axis, 0, 0, tiled=True)


def gather_directly(x, axis, dim):
    return joined_along(from_everyone(x, axis), dim)


def in_one_piece(arrays, axis, dim, along):
    ends, at = ([], 0)
    for a in arrays[:-1]:
        at += a.shape[along]
        ends.append(at)
    both = jnp.concatenate(arrays, axis=along)
    return tuple(jnp.split(gather_directly(both, axis, dim), ends, axis=along))


def normalize(row_values, gain_vector):
    widened = row_values.astype(jnp.float32)
    return (
        widened
        * lax.rsqrt(jnp.mean(widened * widened, axis=-1, keepdims=True) + 1e-05)
        * gain_vector.astype(jnp.float32)
    )


def angles_for(positions, rope_width):
    half_width = rope_width // 2
    inverse = 10000.0 ** (-jnp.arange(half_width, dtype=jnp.float32) / half_width)
    return positions.astype(jnp.float32)[:, None] * inverse[None, :]


def turn(vectors, angles):
    half_width = vectors.shape[-1] // 2
    cosine = jnp.cos(angles)
    sine_value = jnp.sin(angles)
    low_half = vectors[..., :half_width]
    high_half = vectors[..., half_width:]
    return jnp.concatenate(
        [low_half * cosine - high_half * sine_value, high_half * cosine + low_half * sine_value],
        axis=-1,
    )


def attend(query_head, keyval_head, rope_all):
    length = query_head.shape[0]
    local_heads = query_head.shape[1] // (NOPE + ROPE)
    query_three = query_head.reshape(length, local_heads, NOPE + ROPE)
    keyval_three = keyval_head.reshape(length, local_heads, NOPE + VDIM)
    block_rows = min(512, length)
    score_scale = (NOPE + ROPE) ** (-0.5)
    pieces = []
    for block_index in range(length // block_rows):
        block_start = block_index * block_rows
        block_stop = block_start + block_rows
        query_block = query_three[block_start:block_stop]
        scores = jnp.einsum(
            "qhd,khd->hqk",
            query_block[..., :NOPE],
            keyval_three[:block_stop, :, :NOPE],
            preferred_element_type=jnp.float32,
        )
        scores = scores + jnp.einsum(
            "qhr,kr->hqk",
            query_block[..., NOPE:],
            rope_all[:block_stop],
            preferred_element_type=jnp.float32,
        )
        scores = scores * score_scale
        allowed = jnp.arange(block_stop)[None, :] <= (block_start + jnp.arange(block_rows))[:, None]
        scores = jnp.where(allowed[None], scores, -jnp.inf)
        row_top = jnp.max(scores, axis=-1, keepdims=True)
        exponent = jnp.exp(scores - row_top)
        row_total = jnp.sum(exponent, axis=-1)
        summed = jnp.einsum(
            "hqk,khd->qhd",
            exponent.astype(jnp.bfloat16),
            keyval_three[:block_stop, :, NOPE:],
            preferred_element_type=jnp.float32,
        )
        pieces.append((summed / jnp.transpose(row_total)[:, :, None]).astype(jnp.bfloat16))
    return jnp.concatenate(pieces, axis=0).reshape(length, local_heads * VDIM)


def per_device(
    q_latent, kv_latent, rope_key, w_query, w_keyval, w_out, query_gain, latent_gain, out_gain
):
    tokens_here = q_latent.shape[1]
    offset = lax.axis_index("sp") * tokens_here
    positions = offset + jnp.arange(tokens_here, dtype=jnp.int32)
    angles = angles_for(positions, ROPE)
    query_norm = normalize(q_latent[0], query_gain).astype(jnp.bfloat16)
    query_raw = jnp.dot(query_norm, gather_axes(w_query, DP, 1), preferred_element_type=jnp.float32)
    query_raw = query_raw.reshape(tokens_here, H, NOPE + ROPE)
    queries = jnp.concatenate(
        [query_raw[..., :NOPE], turn(query_raw[..., NOPE:], angles[:, None, :])], axis=-1
    )
    queries = queries.astype(jnp.bfloat16).reshape(tokens_here, H * (NOPE + ROPE))
    latent_norm = normalize(kv_latent[0], latent_gain).astype(jnp.bfloat16)
    rope_turned = turn(rope_key[0].astype(jnp.float32), angles).astype(jnp.bfloat16)
    query_head = lax.all_to_all(queries, "sp", split_axis=1, concat_axis=0, tiled=True)
    latent_all, rope_all = in_one_piece((latent_norm, rope_turned), "sp", 0, 1)
    keyval_head = jnp.dot(latent_all, w_keyval, preferred_element_type=jnp.float32).astype(
        jnp.bfloat16
    )
    attended = attend(query_head, keyval_head, rope_all)
    returned = lax.all_to_all(attended, "sp", split_axis=0, concat_axis=1, tiled=True)
    mixed_norm = normalize(returned, out_gain).astype(jnp.bfloat16)
    result = jnp.dot(mixed_norm, w_out, preferred_element_type=jnp.float32).astype(jnp.bfloat16)
    return result[None]


def solution(mesh):
    split = Mesh(mesh.devices.reshape(mesh.shape["sp"], 12, 4), ("sp", "dp_0", "dp_1"))
    placed = (
        P(DP, "sp", None),
        P(DP, "sp", None),
        P(DP, "sp", None),
        P(None, DP),
        P(None, "sp"),
        P(),
        P(),
        P(),
        P(),
    )
    return jax.shard_map(
        per_device, mesh=split, in_specs=placed, out_specs=P(DP, "sp", None), check_vma=False
    )
```

profile of v0, /device:TPU:1, one launch (start us, length us, event | category | flops | bytes accessed | tf_op | source)
XLA Modules:
  0.0 175.0 jit_solution(9191587094716798942)
XLA Ops:
  6.5 12.5 %all_gather.6 = bf16[512,256]{0,1:T(8,128)(2,1)} all-gather(bf16[512,64]{0,1:T(8,128)(2,1)} %param.12), channel_id=1, replica_groups=mesh['sp'=16,'dp_0'=12,'dp_1'=4] {'dp_1'}, dimensions={1}, use_global_device_ids=true | all-gather | bytes 327680 | tf_op jit(solution)/shard_map/all_gather | solution.py:17
  19.1 0.7 bitcast_convert_fusion
  19.8 0.1 multiply_cosine_fusion
  20.0 0.1 copy.44
  20.1 0.1 copy.45
  20.2 0.7 convert_element_type.106
  20.9 1.0 fusion.71
  22.0 1.0 fusion.73
  23.1 0.1 copy.46
  23.2 1.9 %broadcast_in_dim.17 = bf16[16,128,576]{1,2,0:T(8,128)(2,1)} broadcast(bf16[128,576]{0,1:T(8,128)(2,1)S(1)} %copy.46), dimensions={1,2} | broadcast | bytes 2506752 | tf_op jit(solution)/shard_map/broadcast_in_dim | solution.py:29
  25.1 14.9 %all-to-all-start = ((bf16[16,128,576]{1,2,0:T(8,128)(2,1)}), bf16[16,128,576]{1,2,0:T(8,128)(2,1)S(1)}, u32[]{:S(2)}, u32[]{:S(2)}) async-start(bf16[16,128,576]{1,2,0:T(8,128)(2,1)} %broadcast_in_dim.17), calls=%async_computation | async-start | bytes 4718592 | tf_op jit(solution)/shard_map/all_to_all | solution.py:29
  40.1 0.1 fusion.68
  40.2 43.9 %all-gather.2.cloned.1.call-done = bf16[512,3072]{0,1:T(8,128)(2,1)} async-done(((bf16[512,256]{0,1:T(8,128)(2,1)}), bf16[512,3072]{0,1:T(8,128)(2,1)}) %all-gather.2.cloned.1.call-update) | async-done | bytes 3145744 | tf_op jit(solution)/shard_map/all_gather | solution.py:17
  84.1 2.9 %fusion.78 = f32[128,16,192]{0,2,1:T(8,128)S(1)} fusion(bf16[16,192,512]{2,1,0:T(8,128)(2,1)} %bitcast.222, bf16[1,128,512]{2,1,0:T(8,128)(2,1)S(1)} %copy-done.2, f32[512]{0:T(512)S(1)} %convert_element_type.113, f32[128]{0:T(128)S(1)} %add_rsqrt_fusion.1), kind=kOutput, calls=%fused_computation.95 | convolution fusion | flops 402915328 | bytes 4852224 | tf_op jit(solution)/shard_map/dot_general | solution.py:120
  87.2 1.0 pad_maximum_fusion
  88.2 6.2 %all-to-all-done = bf16[16,128,576]{1,2,0:T(8,128)(2,1)S(1)} async-done(((bf16[16,128,576]{1,2,0:T(8,128)(2,1)}), bf16[16,128,576]{1,2,0:T(8,128)(2,1)S(1)}, u32[]{:S(2)}, u32[]{:S(2)}) %all-to-all-start) | async-done | bytes 2359328 | tf_op jit(solution)/shard_map/all_to_all | solution.py:29
  94.4 8.7 %all-to-all-start.1 = ((bf16[128,16,192]{0,2,1:T(8,128)(2,1)}), bf16[128,16,192]{0,2,1:T(8,128)(2,1)S(1)}, u32[]{:S(2)}, u32[]{:S(2)}) async-start(bf16[128,16,192]{0,2,1:T(8,128)(2,1)} %pad_maximum_fusion), calls=%async_computation.1 | async-start | bytes 1572864 | tf_op jit(solution)/shard_map/all_to_all | solution.py:128
  103.2 0.3 copy_bitcast_fusion
  103.5 1.4 copy-done.1
  104.9 0.8 fusion.9
  105.7 20.2 %all-to-all-done.1 = bf16[128,16,192]{0,2,1:T(8,128)(2,1)S(1)} async-done(((bf16[128,16,192]{0,2,1:T(8,128)(2,1)}), bf16[128,16,192]{0,2,1:T(8,128)(2,1)S(1)}, u32[]{:S(2)}, u32[]{:S(2)}) %all-to-all-start.1) | async-done | bytes 786464 | tf_op jit(solution)/shard_map/all_to_all | solution.py:128
  125.9 0.2 copy.48
  126.2 0.3 convolution_bitcast_fusion.2
  126.4 1.2 fusion.88
  127.6 0.2 fusion.62
  127.8 0.3 fusion.56
  128.1 0.2 copy.50
  128.4 0.5 fusion.75
  128.8 1.6 fusion.87
  130.5 0.5 fusion.18
  131.0 0.6 fusion.53
  131.6 0.2 copy.53
  131.9 0.6 convolution_bitcast_fusion.1
  132.5 1.9 %fusion.86 = (f32[512]{0:T(512)S(1)}, f32[1,512,1536]{2,1,0:T(8,128)S(1)}) fusion(f32[1,512,1536]{2,1,0:T(8,128)S(1)} %convolution_bitcast_fusion.1, bf16[512,1,192]{0,2,1:T(8,128)(2,1)S(1)} %slice.124, bf16[2048,576]{0,1:T(8,128)(2,1)} %copy-done.1, s32[512]{0:T(512)S(1)} %iota_add_fusion.1), kind=kOutput, calls=%fused_computation.125 | convolution fusion | flops 104594944 | bytes 6557696 | tf_op jit(solution)/shard_map/qhr,kr->hqk/dot_general | solution.py:90
  134.4 0.6 fusion.7
  134.9 0.8 fusion.45
  135.7 0.2 copy.56
  136.0 0.7 fusion.66
  136.7 2.2 %fusion.85 = (f32[512]{0:T(512)S(1)}, f32[1,512,2048]{2,1,0:T(8,128)S(1)}) fusion(bf16[512,1,192]{0,2,1:T(8,128)(2,1)S(1)} %slice.131, bf16[2048,576]{0,1:T(8,128)(2,1)} %copy-done.1, f32[512,2048]{1,0:T(8,128)S(1)} %fusion.66, s32[512]{0:T(512)S(1)} %iota_add_fusion), kind=kOutput, calls=%fused_computation.124 | convolution fusion | flops 139460096 | bytes 8720384 | tf_op jit(solution)/shard_map/qhr,kr->hqk/dot_general | solution.py:90
  138.9 0.7 fusion.2
  139.7 1.0 fusion.48
  140.7 0.1 copy.64
  140.8 0.9 copy.59
  141.7 3.5 %all-to-all-start.2 = ((bf16[16,128,128]{1,2,0:T(8,128)(2,1)}), bf16[16,128,128]{1,2,0:T(8,128)(2,1)S(1)}, u32[]{:S(2)}, u32[]{:S(2)}) async-start(bf16[16,128,128]{1,2,0:T(8,128)(2,1)} %copy.59), calls=%async_computation.2 | async-start | bytes 1048576 | tf_op jit(solution)/shard_map/all_to_all | solution.py:134
  145.2 16.8 %all-to-all-done.2 = bf16[16,128,128]{1,2,0:T(8,128)(2,1)S(1)} async-done(((bf16[16,128,128]{1,2,0:T(8,128)(2,1)}), bf16[16,128,128]{1,2,0:T(8,128)(2,1)S(1)}, u32[]{:S(2)}, u32[]{:S(2)}) %all-to-all-start.2) | async-done | bytes 524320 | tf_op jit(solution)/shard_map/all_to_all | solution.py:134
  162.0 0.3 multiply_reduce_fusion
  162.3 0.3 fusion.60
  162.7 5.5 %fusion.10 = bf16[1,128,2048]{2,1,0:T(8,128)(2,1)} fusion(bf16[128,2048]{0,1:T(8,128)(2,1)S(1)} %fusion.60, bf16[2048,2048]{1,0:T(8,128)(2,1)} %param.14), kind=kOutput, calls=%fused_computation.20 | convolution fusion | flops 1074003968 | bytes 9437184 | tf_op jit(solution)/shard_map/dot_general | solution.py:136
  (30 shorter events, 0.8 us)
Async XLA Ops:
  6.5 98.4 %copy-start = (bf16[512,256]{1,0:T(8,128)(2,1)S(1)}, bf16[512,256]{1,0:T(8,128)(2,1)}, u32[]{:S(2)}) copy-start(bf16[512,256]{1,0:T(8,128)(2,1)} %param.13) | copy-start | bytes 786436
  6.5 77.6 %all-gather.2.cloned.1.call-start = ((), (), s32[]{:S(2)}) async-start(), calls=%async_computation.3 | async-start | bytes 3407872 | tf_op jit(solution)/shard_map/all_gather | solution.py:17
  25.1 14.9 %copy-start.4 = (bf16[512]{0:T(512)(128)(2,1)S(1)}, bf16[512]{0:T(512)(128)(2,1)}, u32[]{:S(2)}) copy-start(bf16[512]{0:T(512)(128)(2,1)} %param.15) | copy-start | bytes 3076
  25.1 14.9 %copy-start.2 = (bf16[1,128,512]{2,1,0:T(8,128)(2,1)S(1)}, bf16[1,128,512]{2,1,0:T(8,128)(2,1)}, u32[]{:S(2)}) copy-start(bf16[1,128,512]{2,1,0:T(8,128)(2,1)} %param.9) | copy-start | bytes 393220
  25.1 69.3 %all-to-all-start = ((bf16[16,128,576]{1,2,0:T(8,128)(2,1)}), bf16[16,128,576]{1,2,0:T(8,128)(2,1)S(1)}, u32[]{:S(2)}, u32[]{:S(2)}) async-start(bf16[16,128,576]{1,2,0:T(8,128)(2,1)} %broadcast_in_dim.17), calls=%async_computation | async-start | bytes 4718592 | tf_op jit(solution)/shard_map/all_to_all | solution.py:29
  94.4 31.4 %all-to-all-start.1 = ((bf16[128,16,192]{0,2,1:T(8,128)(2,1)}), bf16[128,16,192]{0,2,1:T(8,128)(2,1)S(1)}, u32[]{:S(2)}, u32[]{:S(2)}) async-start(bf16[128,16,192]{0,2,1:T(8,128)(2,1)} %pad_maximum_fusion), calls=%async_computation.1 | async-start | bytes 1572864 | tf_op jit(solution)/shard_map/all_to_all | solution.py:128
  103.5 1.4 copy-start.1
  140.6 4.6 %copy-start.3 = (bf16[2048]{0:T(1024)(128)(2,1)S(1)}, bf16[2048]{0:T(1024)(128)(2,1)}, u32[]{:S(2)}) copy-start(bf16[2048]{0:T(1024)(128)(2,1)} %param.17) | copy-start | bytes 12292
  141.7 20.3 %all-to-all-start.2 = ((bf16[16,128,128]{1,2,0:T(8,128)(2,1)}), bf16[16,128,128]{1,2,0:T(8,128)(2,1)S(1)}, u32[]{:S(2)}, u32[]{:S(2)}) async-start(bf16[16,128,128]{1,2,0:T(8,128)(2,1)} %copy.59), calls=%async_computation.2 | async-start | bytes 1048576 | tf_op jit(solution)/shard_map/all_to_all | solution.py:134
Sparse Core Ops, SparseCore 0:
  19.2 64.8 all-gather.1
where the time goes:
time: 176 us; the launch traced here: 175 us
  waiting for transfers between devices  87.1 us (49%)
  starting transfers between devices  27.1 us (15%)
  matrix products  20.8 us (12%)
  between operations  13.7 us (8%)
  blocking collectives  12.5 us (7%)
  other arithmetic  7.55 us (4%)
  local copies, waits for them, and re-layouts  6.2 us (4%)
    all_gather x1, waiting for transfers between devices, gather_axes(): nearer = lax.all_gather(x, axes[-1], axis=dim, tiled=True)  43.9 us
    all_to_all x1, waiting for transfers between devices, per_device(): lax.all_to_all(queries, 'sp', split_axis=1, concat_axis=0, tiled=True)  20.2 us
    all_to_all x1, waiting for transfers between devices, per_device(): lax.all_to_all(attended, 'sp', split_axis=0, concat_axis=1, tiled=True)  16.8 us
    all_to_all x1, starting transfers between devices, from_everyone(): lax.all_to_all(jnp.broadcast_to(x[None], (peers, *x.shape)), axis, 0, 0,...  14.9 us
    all_gather x1, blocking collectives, gather_axes(): nearer = lax.all_gather(x, axes[-1], axis=dim, tiled=True)  12.5 us
    all_to_all x1, starting transfers between devices, per_device(): lax.all_to_all(queries, 'sp', split_axis=1, concat_axis=0, tiled=True)  8.7 us
    dot_general x4, matrix products, attend(): jnp.einsum('qhr,kr->hqk', query_block[..., NOPE:], rope_all[:block_stop],...  6.96 us
    all_to_all x1, waiting for transfers between devices, from_everyone(): lax.all_to_all(jnp.broadcast_to(x[None], (peers, *x.shape)), axis, 0, 0,...  6.22 us
  transfers between devices with their start and end apart: 4, of which 4 were waited for; matrix products, arithmetic and copies ran while one was open for 6% of the time, Pallas kernels for 0%

commit v1 on v0

v1 whole, which is shorter than its diff:
```python
import functools
import math

import jax
import jax.numpy as jnp
import numpy as np
from jax import lax
from jax.experimental import pallas as pl
from jax.experimental.pallas import tpu as pltpu
from jax.sharding import PartitionSpec as P

H = 16
NOPE = 128
ROPE = 64
VDIM = 128
D = 2048
SP = 16
CHIPS = SP // 2
NX = 4
ROWS = 128
LAT = 512
KV_ROWS = 144
MSG_ROWS = KV_ROWS + ROWS
CUT = 80
EPS = 1e-05
EXPONENT = (NOPE + ROPE) ** (-0.5) * math.log2(math.e)
BF16 = jnp.bfloat16
F32 = jnp.float32
MESH = pl.DeviceIdType.MESH


def rotary_tables():
    inverse = np.float32(10000.0) ** (-np.arange(32, dtype=np.float32) / np.float32(32))

    def both(positions):
        angles = positions.astype(np.float64)[:, None] * inverse.astype(np.float64)[None, :]
        return np.cos(angles), np.sin(angles)

    far_cos, far_sin = both(np.arange(SP) * ROWS)
    near_cos, near_sin = both(np.arange(ROWS))
    u = np.concatenate([far_cos, far_cos, -far_sin, far_sin], axis=1)
    v = np.concatenate([-far_sin, -far_sin, -far_cos, far_cos], axis=1)
    c = np.concatenate([near_cos] * 4, axis=1)
    s = np.concatenate([near_sin] * 4, axis=1)
    return np.concatenate([u, v, c, s], axis=0).astype(np.float32)


def selection(shape, pairs):
    row = lax.broadcasted_iota(jnp.int32, shape, 0)
    column = lax.broadcasted_iota(jnp.int32, shape, 1)
    hit = None
    for row_from, column_from, width in pairs:
        here = (
            (column >= column_from)
            & (column < column_from + width)
            & (column - column_from == row - row_from)
        )
        hit = here if hit is None else hit | here
    return jnp.where(hit, 1.0, 0.0).astype(BF16)


def dot(a, b):
    return jnp.dot(a, b, preferred_element_type=F32)


def normalized(x, gain):
    wide = x.astype(F32)
    mean = jnp.mean(wide * wide, axis=-1, keepdims=True)
    return (wide * lax.rsqrt(mean + EPS) * gain.astype(F32)).astype(BF16)


def kernel(
    nz,
    q_in,
    kv_in,
    rope_in,
    wq_in,
    wkv_in,
    wout_in,
    qg_ref,
    lg_ref,
    og_ref,
    tab_in,
    out_ref,
    xq,
    xkv,
    xr,
    xw,
    wkv,
    wout,
    tab,
    msg,
    ws,
    wext,
    kx,
    vx,
    att,
    rcv,
    acc,
    outv,
    ogain,
    load_sem,
    ring_send,
    ring_recv,
    sib_send,
    sib_recv,
    ret_send,
    ret_recv,
    wz_send,
    wx_send,
    w_recv,
):
    s = lax.axis_index("sp")
    y = s // 2
    sib = s + 1 - 2 * lax.rem(s, 2)
    right = lax.rem(s + 2, SP)
    left = lax.rem(s + SP - 2, SP)
    spread = nz > 1
    if spread:
        dp = lax.axis_index("dp")
        z = dp // NX
        x = lax.rem(dp, NX)

    barrier = pltpu.get_barrier_semaphore()
    greeted = 0
    for step in range(1, SP):
        pl.semaphore_signal(
            barrier, inc=1, device_id={"sp": lax.rem(s + step, SP)}, device_id_type=MESH
        )
        greeted += 1
    if spread:
        for step in range(1, nz):
            pl.semaphore_signal(
                barrier,
                inc=1,
                device_id={"dp": lax.rem(z + step, nz) * NX + x},
                device_id_type=MESH,
            )
            greeted += 1
        for step in range(1, NX):
            pl.semaphore_signal(
                barrier,
                inc=1,
                device_id={"dp": z * NX + lax.rem(x + step, NX)},
                device_id_type=MESH,
            )
            greeted += 1

    loads = [
        pltpu.make_async_copy(source, target, load_sem.at[i])
        for i, (source, target) in enumerate(
            [
                (kv_in, xkv),
                (rope_in, xr),
                (tab_in, tab),
                (q_in, xq),
                (wq_in, xw),
                (wkv_in, wkv),
                (wout_in, wout),
            ]
        )
    ]
    for load in loads:
        load.start()

    def turning(slot):
        return (
            tab[pl.ds(slot, 1), :] * tab[2 * SP : 2 * SP + ROWS, :]
            + tab[pl.ds(SP + slot, 1), :] * tab[2 * SP + ROWS :, :]
        )

    def turned(halves, slot):
        products = halves * turning(slot)
        return products + pltpu.roll(products, 64, 1)

    low_lanes = lax.broadcasted_iota(jnp.int32, (ROWS // 2, 128), 1) < 64

    loads[0].wait()
    msg[s, 0:ROWS, :] = normalized(xkv[...], lg_ref[...])
    loads[1].wait()
    loads[2].wait()
    swap = selection((64, 128), [(0, 0, 64), (32, 64, 32), (0, 96, 32)])
    rope = turned(dot(xr[...], swap), s)
    folded = jnp.where(low_lanes, rope[: ROWS // 2], rope[ROWS // 2 :]).astype(BF16)
    for i in range(4):
        msg[s, ROWS:KV_ROWS, 128 * i : 128 * (i + 1)] = folded[16 * i : 16 * (i + 1)]
    loads[3].wait()
    msg[s, KV_ROWS:, :] = normalized(xq[...], qg_ref[...])

    loads[4].wait()
    left_half = selection((64, 128), [(0, 0, 64)])
    right_half = selection((64, 128), [(0, 64, 64)])

    def folded_weight(w):
        return (dot(w[:256], left_half) + dot(w[256:], right_half)).astype(BF16)

    if spread:
        third = lax.rem(x + s, NX)
        carries = third < 3
        own_third = lax.rem(third, 3)
        is_source = carries & (dp == 3 * s + third)

        @pl.when(is_source)
        def _():
            ws[own_third] = folded_weight(xw[...])

    else:
        for i in range(3):
            ws[i] = folded_weight(xw[:, 64 * i : 64 * (i + 1)])

    pl.semaphore_wait(barrier, greeted)

    part_rows = ((0, KV_ROWS), (KV_ROWS, MSG_ROWS))
    half_rows = (((0, CUT), (KV_ROWS, KV_ROWS + 64)), ((CUT, KV_ROWS), (KV_ROWS + 64, MSG_ROWS)))

    def ring_copy(direction, step, part):
        slot = lax.rem(s + SP - 2 * step, SP) if direction == 0 else lax.rem(s + 2 * step, SP)
        lo, hi = part_rows[part] if step < 3 else half_rows[direction][part]
        piece = msg.at[slot, pl.ds(lo, hi - lo), :]
        return pltpu.make_async_remote_copy(
            src_ref=piece,
            dst_ref=piece,
            send_sem=ring_send.at[direction, step, part],
            recv_sem=ring_recv.at[direction, step, part],
            device_id={"sp": right if direction == 0 else left},
            device_id_type=MESH,
        )

    def ring_arrival(direction, step, part):
        slot = lax.rem(s + SP - 2 * step, SP) if direction == 0 else lax.rem(s + 2 * step, SP)
        lo, hi = part_rows[part] if step < 4 else half_rows[direction][part]
        piece = msg.at[slot, pl.ds(lo, hi - lo), :]
        return pltpu.make_async_remote_copy(
            src_ref=piece,
            dst_ref=piece,
            send_sem=ring_send.at[direction, step - 1, part],
            recv_sem=ring_recv.at[direction, step - 1, part],
            device_id={"sp": right if direction == 0 else left},
            device_id_type=MESH,
        )

    def item_of(direction, step):
        if step == 0:
            return 0
        return 1 + 3 * direction + step - 1 if step < 4 else 7 + direction

    def sib_copy(direction, step, part, mine=True):
        base = s if mine else sib
        slot = lax.rem(base + SP - 2 * step, SP) if direction == 0 else lax.rem(base + 2 * step, SP)
        lo, hi = part_rows[part] if step < 4 else half_rows[direction][part]
        piece = msg.at[slot, pl.ds(lo, hi - lo), :]
        item = item_of(direction, step)
        return pltpu.make_async_remote_copy(
            src_ref=piece,
            dst_ref=piece,
            send_sem=sib_send.at[item, part],
            recv_sem=sib_recv.at[item, part],
            device_id={"sp": sib},
            device_id_type=MESH,
        )

    sends = []

    def start(copy):
        copy.start()
        sends.append(copy)

    for part in range(2):
        for direction in range(2):
            start(ring_copy(direction, 0, part))
        start(sib_copy(0, 0, part))

    def z_copy(step):
        return pltpu.make_async_remote_copy(
            src_ref=ws.at[own_third],
            dst_ref=ws.at[own_third],
            send_sem=wz_send.at[step - 1],
            recv_sem=w_recv.at[own_third],
            device_id={"dp": lax.rem(z + step, nz) * NX + x},
            device_id_type=MESH,
        )

    def x_copy(step):
        return pltpu.make_async_remote_copy(
            src_ref=ws.at[own_third],
            dst_ref=ws.at[own_third],
            send_sem=wx_send.at[step - 1],
            recv_sem=w_recv.at[own_third],
            device_id={"dp": z * NX + lax.rem(x + step, NX)},
            device_id_type=MESH,
        )

    def w_arrival(i):
        return pltpu.make_async_remote_copy(
            src_ref=ws.at[i],
            dst_ref=ws.at[i],
            send_sem=wx_send.at[0],
            recv_sem=w_recv.at[i],
            device_id={"sp": sib},
            device_id_type=MESH,
        )

    if spread:

        @pl.when(is_source)
        def _():
            for step in (6, 5, 7, 4, 8, 3, 9, 2, 10, 1, 11):
                z_copy(step).start()

    def project(slot):
        keyval = dot(msg[slot, 0:ROWS, :], wkv[...])
        at = pl.ds(pl.multiple_of(slot * ROWS, ROWS), ROWS)
        kx[at, 0:NOPE] = keyval[:, :NOPE].astype(BF16)
        vx[at, :] = keyval[:, NOPE:].astype(BF16)
        rope_tile = jnp.concatenate(
            [msg[slot, ROWS:KV_ROWS, 128 * i : 128 * (i + 1)] for i in range(4)], axis=0
        ).astype(F32)
        upper = pl.ds(pl.multiple_of(slot * ROWS, ROWS), ROWS // 2)
        lower = pl.ds(pl.multiple_of(slot * ROWS + ROWS // 2, ROWS // 2), ROWS // 2)
        kx[upper, NOPE:] = jnp.where(low_lanes, rope_tile, 0.0).astype(BF16)
        kx[lower, NOPE:] = jnp.where(low_lanes, 0.0, rope_tile).astype(BF16)

    loads[5].wait()
    project(s)
    sib_copy(0, 0, 0, mine=False).wait_recv()
    project(sib)

    for step in range(1, 5):
        for part in range(2):
            for direction in range(2):
                ring_arrival(direction, step, part).wait_recv()
                if step < 4:
                    start(ring_copy(direction, step, part))
                start(sib_copy(direction, step, part))
            if part == 0 and step < 4:
                for direction in range(2):
                    project(
                        lax.rem(s + SP - 2 * step, SP)
                        if direction == 0
                        else lax.rem(s + 2 * step, SP)
                    )
                    sib_copy(direction, step, part, mine=False).wait_recv()
                    project(
                        lax.rem(sib + SP - 2 * step, SP)
                        if direction == 0
                        else lax.rem(sib + 2 * step, SP)
                    )
            if part == 0 and step == 4:
                project(lax.rem(s + SP // 2, SP))
                for direction in range(2):
                    sib_copy(direction, step, part, mine=False).wait_recv()
                project(lax.rem(sib + SP // 2, SP))
        if step == 2 and spread:

            @pl.when(carries)
            def _():
                @pl.when(jnp.logical_not(is_source))
                def _():
                    w_arrival(own_third).wait_recv()

                for hop in range(1, NX):
                    x_copy(hop).start()

        if step == 3:
            if spread:
                for i in range(3):

                    @pl.when(jnp.logical_or(jnp.logical_not(carries), own_third != i))
                    def _():
                        w_arrival(i).wait_recv()

            take = [
                selection((128, 256), [(0, 0, 64)]),
                selection((128, 256), [(0, 64, 64)]),
                selection((128, 256), [(0, 128, 64), (32, 192, 32), (0, 224, 32)]),
                selection((128, 256), [(64, 0, 64)]),
                selection((128, 256), [(64, 64, 64)]),
                selection((128, 256), [(64, 128, 64), (96, 192, 32), (64, 224, 32)]),
            ]
            for half in range(2):
                wext[256 * half : 256 * (half + 1), :] = (
                    dot(ws[0], take[3 * half])
                    + dot(ws[1], take[3 * half + 1])
                    + dot(ws[2], take[3 * half + 2])
                ).astype(BF16)

    for step in range(5):
        for direction in range(2):
            if step > 0 or direction == 0:
                sib_copy(direction, step, 1, mine=False).wait_recv()

    def ret_copy(target):
        return pltpu.make_async_remote_copy(
            src_ref=att.at[target],
            dst_ref=rcv.at[s],
            send_sem=ret_send.at[target],
            recv_sem=ret_recv.at[s],
            device_id={"sp": target},
            device_id_type=MESH,
        )

    def ret_arrival(source):
        return pltpu.make_async_remote_copy(
            src_ref=att.at[source],
            dst_ref=rcv.at[source],
            send_sem=ret_send.at[source],
            recv_sem=ret_recv.at[source],
            device_id={"sp": sib},
            device_id_type=MESH,
        )

    def away(i):
        order = (0, 3, 5, 4, 2, 6, 1, 7)
        value = order[7]
        for n in range(6, -1, -1):
            value = jnp.where(i == n, order[n], value)
        return value

    def attend(chip, reach):
        rows = 2 * ROWS
        raw = dot(msg[pl.ds(2 * chip, 2), KV_ROWS:, :].reshape(rows, LAT), wext[...])
        rotary = jnp.concatenate(
            [
                turned(raw[:ROWS, NOPE:], 2 * chip),
                turned(raw[ROWS:, NOPE:], 2 * chip + 1),
            ],
            axis=0,
        )
        query = jnp.concatenate([raw[:, :NOPE].astype(BF16), rotary.astype(BF16)], axis=1)
        stop = 512 * (reach + 1)
        scores = lax.dot_general(
            query, kx[0:stop, :], (((1,), (1,)), ((), ())), preferred_element_type=F32
        )
        position = chip * rows + lax.broadcasted_iota(jnp.int32, (rows, 512), 0)
        key = stop - 512 + lax.broadcasted_iota(jnp.int32, (rows, 512), 1)
        last = jnp.where(key <= position, scores[:, stop - 512 :], -jnp.inf)
        top = jnp.max(last, axis=-1, keepdims=True)
        if reach > 0:
            top = jnp.maximum(top, jnp.max(scores[:, : stop - 512], axis=-1, keepdims=True))
        weight = jnp.exp2((last - top) * EXPONENT)
        total = jnp.sum(weight, axis=-1, keepdims=True)
        summed = dot(weight.astype(BF16), vx[stop - 512 : stop, :])
        if reach > 0:
            weight = jnp.exp2((scores[:, : stop - 512] - top) * EXPONENT)
            total = total + jnp.sum(weight, axis=-1, keepdims=True)
            summed = summed + dot(weight.astype(BF16), vx[0 : stop - 512, :])
        attended = (summed / total).astype(BF16)
        att[2 * chip] = attended[:ROWS]
        att[2 * chip + 1] = attended[ROWS:]

    def attend_step(i, carry):
        chip = lax.rem(y + away(i), CHIPS)
        for reach in range(4):

            @pl.when(chip // 2 == reach)
            def _():
                attend(chip, reach)

        @pl.when(i == 0)
        def _():
            rcv[s] = att[s]
            ret_copy(sib).start()

        @pl.when(i > 0)
        def _():
            ret_copy(2 * chip).start()
            ret_copy(2 * chip + 1).start()

        return carry

    lax.fori_loop(0, CHIPS, attend_step, 0)

    acc[...] = jnp.zeros_like(acc)
    ogain[...] = og_ref[...].astype(F32)
    loads[6].wait()

    def out_step(i, squares):
        chip = lax.rem(y + CHIPS - away(i), CHIPS)
        for core in range(2):

            @pl.when(2 * chip + core != s)
            def _():
                ret_arrival(2 * chip + core).wait_recv()

        heads = jnp.concatenate([rcv[2 * chip], rcv[2 * chip + 1]], axis=1).astype(F32)
        gained = (heads * ogain[pl.ds(chip, 1), :]).astype(BF16)
        acc[...] += dot(gained, wout[pl.ds(pl.multiple_of(chip * 256, 256), 256), :])
        return squares + jnp.sum(heads * heads, axis=-1, keepdims=True)

    squares = lax.fori_loop(0, CHIPS, out_step, jnp.zeros((ROWS, 1), F32))
    outv[...] = (acc[...] * lax.rsqrt(squares * (1.0 / D) + EPS)).astype(BF16)
    store = pltpu.make_async_copy(outv, out_ref, load_sem.at[7])
    store.start()

    for copy in sends:
        copy.wait_send()
    for step in range(1, SP):
        ret_copy(lax.rem(s + step, SP)).wait_send()
    if spread:

        @pl.when(is_source)
        def _():
            for step in range(1, nz):
                z_copy(step).wait_send()

        @pl.when(carries)
        def _():
            for hop in range(1, NX):
                x_copy(hop).wait_send()

    store.wait()


def per_device(
    nz, q_latent, kv_latent, rope_key, w_query, w_keyval, w_out, query_gain, latent_gain, out_gain
):
    anywhere = pl.BlockSpec(memory_space=pl.ANY)
    local = pl.BlockSpec(memory_space=pltpu.VMEM)
    dma = pltpu.SemaphoreType.DMA
    result = pl.pallas_call(
        functools.partial(kernel, nz),
        out_shape=jax.ShapeDtypeStruct((ROWS, D), BF16),
        in_specs=[anywhere] * 6 + [local] * 3 + [anywhere],
        out_specs=anywhere,
        scratch_shapes=[
            pltpu.VMEM((ROWS, LAT), BF16),
            pltpu.VMEM((ROWS, LAT), BF16),
            pltpu.VMEM((ROWS, ROPE), BF16),
            pltpu.VMEM(w_query.shape, BF16),
            pltpu.VMEM((LAT, NOPE + VDIM), BF16),
            pltpu.VMEM((H * VDIM, D), BF16),
            pltpu.VMEM((2 * SP + 2 * ROWS, 128), F32),
            pltpu.VMEM((SP, MSG_ROWS, LAT), BF16),
            pltpu.VMEM((3, 256, 128), BF16),
            pltpu.VMEM((LAT, 256), BF16),
            pltpu.VMEM((SP * ROWS, 256), BF16),
            pltpu.VMEM((SP * ROWS, VDIM), BF16),
            pltpu.VMEM((SP, ROWS, VDIM), BF16),
            pltpu.VMEM((SP, ROWS, VDIM), BF16),
            pltpu.VMEM((ROWS, D), F32),
            pltpu.VMEM((ROWS, D), BF16),
            pltpu.VMEM((CHIPS, 256), F32),
            dma((8,)),
            dma((2, 4, 2)),
            dma((2, 4, 2)),
            dma((9, 2)),
            dma((9, 2)),
            dma((SP,)),
            dma((SP,)),
            dma((11,)),
            dma((3,)),
            dma((3,)),
        ],
        compiler_params=pltpu.CompilerParams(
            collective_id=0, has_side_effects=True, vmem_limit_bytes=60 * 1024 * 1024
        ),
    )(
        q_latent[0],
        kv_latent[0],
        rope_key[0],
        w_query,
        w_keyval,
        w_out,
        query_gain.reshape(1, LAT),
        latent_gain.reshape(1, LAT),
        out_gain.reshape(CHIPS, 256),
        jnp.asarray(rotary_tables()),
    )
    return result[None]


def solution(mesh):
    nz = mesh.shape["dp"] // NX
    rows = P("dp", "sp", None)
    return jax.shard_map(
        functools.partial(per_device, nz),
        mesh=mesh,
        in_specs=(rows, rows, rows, P(None, "dp"), P(None, "sp"), P(), P(), P(), P()),
        out_specs=rows,
        check_vma=False,
    )
```

time: 176 us -> 71.4 us (0.41)
  waiting for transfers between devices: 87.1 us -> 0 us
  Pallas kernels: 0 us -> 62.3 us
  starting transfers between devices: 27.1 us -> 0 us
  matrix products: 20.8 us -> 0 us
  between operations: 13.7 us -> 0.01 us
  blocking collectives: 12.5 us -> 0 us
  other arithmetic: 7.55 us -> 0 us
  local copies, waits for them, and re-layouts: 6.2 us -> 8.71 us
    pallas_call x0 -> x1, Pallas kernels: none -> 62.3 us  [per_device(): pl.pallas_call(functools.partial(kernel, nz), out_shape=jax.ShapeDtypeStr...]
    all_gather x1 -> x0, waiting for transfers between devices: 43.9 us -> none  [gather_axes(): nearer = lax.all_gather(x, axes[-1], axis=dim, tiled=True)]
    all_to_all x3 -> x0, waiting for transfers between devices: 43.1 us -> none  [the longest x1 20.2 us: per_device(): lax.all_to_all(queries, 'sp', split_axis=1, concat_axis=0, tiled=True)]
    all_to_all x3 -> x0, starting transfers between devices: 27.1 us -> none  [the longest x1 14.9 us: from_everyone(): lax.all_to_all(jnp.broadcast_to(x[None], (peers, *x.shape)), axis, 0, 0,...]
    dot_general x15 -> x0, matrix products: 20.8 us -> none  [the longest x4 6.96 us: attend(): jnp.einsum('qhr,kr->hqk', query_block[..., NOPE:], rope_all[:block_stop],...]
    all_gather x1 -> x0, blocking collectives: 12.5 us -> none  [gather_axes(): nearer = lax.all_gather(x, axes[-1], axis=dim, tiled=True)]
    reshape x1 -> x3, local copies, waits for them, and re-layouts: 0.35 us -> 3.81 us  [the longest x1 1.29 us: per_device(): out_gain.reshape(CHIPS, 256)]
    reduce_sum x7 -> x0, other arithmetic: 3.41 us -> none  [the longest x4 2 us: attend(): row_total = jnp.sum(exponent, axis=-1)]
  transfers between devices with their start and end apart: 4 -> 0, of which waited for: 4 -> 0; matrix products, arithmetic and copies ran while one was open for 6% -> 0% of each run, Pallas kernels for 0% -> 0%
where the time goes in v1:
time: 71.4 us; the launch traced here: 71 us
  Pallas kernels  62.3 us (87%)
  local copies, waits for them, and re-layouts  8.71 us (12%)
    pallas_call x1, Pallas kernels, per_device(): pl.pallas_call(functools.partial(kernel, nz), out_shape=jax.ShapeDtypeStr...  62.3 us
    unnamed x3, local copies, waits for them, and re-layouts  4.9 us

profile of v1, /device:TPU:1, one launch (start us, length us, event | category | flops | bytes accessed | tf_op | source)
XLA Modules:
  0.0 71.0 jit_solution(12344714296496132726)
XLA Ops:
  0.0 1.3 %reshape.9.qg_ref = bf16[1,512]{1,0:T(2,128)(2,1)} reshape(bf16[512]{0:T(512)(128)(2,1)} %param.16) | data formatting | bytes 2048 | tf_op jit(solution)/shard_map/reshape | solution.py:564
  1.3 1.3 %reshape.10.lg_ref = bf16[1,512]{1,0:T(2,128)(2,1)} reshape(bf16[512]{0:T(512)(128)(2,1)} %param.17) | data formatting | bytes 2048 | tf_op jit(solution)/shard_map/reshape | solution.py:565
  2.5 1.3 %reshape.11.og_ref = bf16[8,256]{1,0:T(8,128)(2,1)} reshape(bf16[2048]{0:T(1024)(128)(2,1)} %param.18) | data formatting | bytes 8192 | tf_op jit(solution)/shard_map/reshape | solution.py:566
  3.8 1.4 %copy.11 = bf16[1,128,64]{2,1,0:T(8,128)(2,1)} copy(bf16[1,128,64]{1,2,0:T(8,128)(2,1)} %param.12) | data formatting | bytes 32768 | tf_op args[2]
  5.2 1.6 %copy.12.wq_in = bf16[512,64]{1,0:T(8,128)(2,1)} copy(bf16[512,64]{0,1:T(8,128)(2,1)} %param.13) | data formatting | bytes 131072 | tf_op args[3]
  6.8 62.3 %shard_map.100 = bf16[128,2048]{1,0:T(8,128)(2,1)} custom-call(bf16[128,512]{1,0:T(8,128)(2,1)} %bitcast.5, bf16[128,512]{1,0:T(8,128)(2,1)} %bitcast.6, bf16[128,64]{1,0:T(8,128)(2,1)} %bitcast.7, bf16[512,64]{1,0:T(8,128)(2,1)} %copy.12.wq_in, bf16[512,256]{1,0:T(8,128)(2,1)} %wkv_in.1, bf16[2048,2048]{1,0:T(8,128)(2,1)} %wout_in.1, ...), custom_call_target="tpu_custom_call" | custom-call | tf_op jit(solution)/shard_map/pallas_call | solution.py:520
  69.1 1.9 %copy.14 = bf16[1,128,2048]{2,1,0:T(8,128)(2,1)} copy(bf16[1,128,2048]{2,1,0:T(8,128)(2,1)} %bitcast.4) | data formatting | bytes 1048576
